TPU v7x, 32 devices: a whole 2x2x4 slice. The times are simulated.
32 devices in a mesh: ep: 16 (over z, y, core), tp: 2 (over x).
Axes of the slice: x: 2, y: 2, z: 4, core: 2. Of those that a mesh axis runs over, the one named last changes fastest.
Arguments:
- resid: bfloat16 [256, 2048], P('ep'), may hold values from -40 to 40
- queries: bfloat16 [256, 1024], P('ep', 'tp'), may hold values from -146 to 146
- new_keys: bfloat16 [256, 512], P('ep', 'tp'), may hold values from -6 to 6
- new_values: bfloat16 [256, 512], P('ep', 'tp'), may hold values from -18 to 18
- key_cache: bfloat16 [256, 4, 256, 128], P('ep', 'tp'), may hold values from -5 to 5
- value_cache: bfloat16 [256, 4, 256, 128], P('ep', 'tp'), may hold values from -18 to 18
- cum_gate: float32 [256, 8, 256], P('ep', 'tp'), may hold values from -256 to 0, as said below
- forget_logit: float32 [256, 8], P('ep', 'tp'), may hold values from -6 to 6
- forget_bias: float32 [8], P('tp'), may hold values from -3 to 2
- lengths: int32 [256], P('ep'), may hold values from 32 to 256
- out_weight: bfloat16 [1024, 2048], P('tp'), may hold values from -0.1875 to 0.1875
- norm_gain: float32 [2048], replicated, may hold values from 0.1 to 1.9
- mix_vector: bfloat16 [2048], replicated, may hold values from -0.125 to 0.125
- routes: int32 [256, 2], P('ep'), may hold values from 0 to 3, all different within a row; in each aligned block of 16 rows (0 to 15, 16 to 31, ...) at most 16 rows name the same one
- route_weight: float32 [256, 2], P('ep'), may hold values from 0.2 to 1
- expert_gate: bfloat16 [16, 2048, 768], P('ep', 'tp'), may hold values from -0.125 to 0.125
- expert_up: bfloat16 [16, 2048, 768], P('ep', 'tp'), may hold values from -0.125 to 0.125
- expert_down: bfloat16 [16, 768, 2048], P('ep', None, 'tp'), may hold values from -0.109375 to 0.109375
- dense_gate: bfloat16 [2048, 3072], P('tp', 'ep'), may hold values from -0.125 to 0.125
- dense_up: bfloat16 [2048, 3072], P('tp', 'ep'), may hold values from -0.125 to 0.125
- dense_down: bfloat16 [3072, 2048], P('ep', 'tp'), may hold values from -0.109375 to 0.109375
Outputs:
- layer_out: bfloat16 [256, 2048], P('ep', 'tp')
Inputs may be any that keep to these rules, and one draw needn't show every extreme that they name: `routes`: each row names 2 different experts; the rows of one index of ep name no expert more than 16 times. `cum_gate`: for positions below the sequence's length, the running sum of the log forget gates of positions 0 to p; it never rises along p.
All inputs are finite; a program needn't handle non-finite values.
Results may differ from a plain program's by a relative error of at most 0.0095.
Values may be sent and summed in bfloat16 or wider, within the bound.
A program may use at most 64 MiB of HBM per device.

v0:
```python
import functools
import math

import jax
import jax.numpy as jnp
from jax import lax
from jax.experimental import pallas as pl
from jax.experimental.pallas import tpu as pltpu
from jax.sharding import PartitionSpec as P

HEAD = 128
TOP_K = 2
EXP_SPAN = 4


EPSILON = 1e-06
MESH = pl.DeviceIdType.MESH
META = 128
SEG = 42
GROUPS = 8
INNER = 2
ORDER = ((0, 0), (0, 1), (2, 0), (2, 1), (1, 0), (1, 1), (3, 0), (3, 1))
CACHE_CHUNKS = 4
AHEAD = 3
MID_LAG = 2
OUT_LAG = 4
VMEM_LIMIT = 60 * 1024 * 1024


def layer_kernel(
    dims,
    q_ref,
    nk_ref,
    nv_ref,
    cum_ref,
    flogit_ref,
    fbias_ref,
    len_ref,
    resid_ref,
    gain_ref,
    mix_ref,
    routes_ref,
    rw_ref,
    kc_hbm,
    vc_hbm,
    ow_hbm,
    eg_hbm,
    eu_hbm,
    ed_hbm,
    dg_hbm,
    du_hbm,
    dd_hbm,
    out_ref,
    kc,
    vc,
    q_buf,
    nk_buf,
    nv_buf,
    lf_buf,
    len_buf,
    score_buf,
    mix_buf,
    att_buf,
    ow,
    eg,
    eu,
    ed,
    dg,
    du,
    dd,
    pp_send,
    pp_recv,
    state_buf,
    norm_buf,
    gat,
    pf,
    psend,
    precv,
    hid,
    rs_send,
    rs_recv,
    load_sem,
    cache_sem,
    pp_ssem,
    pp_rsem,
    ag_ssem,
    ag_psem,
    fwd_ssem,
    ag_rsem,
    p_ssem,
    p_rsem,
    h_ssem,
    h_rsem,
    rs_ssem,
    rs_rsem,
):
    ep_n, tp_n, groups, order = dims
    ep = lax.axis_index("ep")
    tp = lax.axis_index("tp")
    f32, bf16 = jnp.float32, jnp.bfloat16
    tokens, width = out_ref.shape
    span = eg.shape[1]
    dspan = dg.shape[0]
    chips = ep_n // 2
    cpg = chips // groups
    epg = ep_n // groups
    rows = epg * tokens
    part = rows // tp_n
    chip = ep // 2
    core = lax.rem(ep, 2)
    partner = chip * 2 + 1 - core
    mygroup = chip // cpg
    inchip = lax.rem(chip, cpg)
    inner = max(1, min(INNER, groups))
    outer = groups // inner

    def place(j):
        high = lax.rem(mygroup // inner + j[0], outer)
        return high * inner + lax.rem(lax.rem(mygroup, inner) + j[1], inner)


    kv_local = kc.shape[1]
    heads = q_buf.shape[1]
    slots = kc.shape[2]
    grouping = heads // kv_local
    step = tokens // CACHE_CHUNKS
    cache = []
    for side, (src, dst) in enumerate(((kc_hbm, kc), (vc_hbm, vc))):
        for n in range(CACHE_CHUNKS):
            some = pl.ds(n * step, step)
            cache.append(
                pltpu.make_async_copy(src.at[some], dst.at[some], cache_sem.at[side, n])
            )
    for load in cache:
        load.start()
    loads = [
        pltpu.make_async_copy(src, dst, load_sem.at[i])
        for i, (src, dst) in enumerate(
            [
                (ow_hbm, ow),
                (eg_hbm.at[0], eg),
                (eu_hbm.at[0], eu),
                (dg_hbm, dg),
                (du_hbm, du),
                (ed_hbm.at[0], ed),
                (dd_hbm, dd),
            ]
        )
    ]
    loads[0].start()

    barrier = pltpu.get_barrier_semaphore()
    for k in range(1, ep_n):
        pl.semaphore_signal(
            barrier, inc=1, device_id=(lax.rem(ep + k, ep_n), tp), device_id_type=MESH
        )
    for k in range(1, tp_n):
        pl.semaphore_signal(
            barrier, inc=1, device_id=(ep, lax.rem(tp + k, tp_n)), device_id_type=MESH
        )

    eye = lax.broadcasted_iota(jnp.int32, (tokens, tokens), 0) == lax.broadcasted_iota(
        jnp.int32, (tokens, tokens), 1
    )

    def column(row):
        return jnp.sum(jnp.where(eye, row, 0.0), axis=1, keepdims=True)

    for h in range(heads):
        g = h // grouping
        q_buf[:, h, :] = q_ref[:, h * HEAD : (h + 1) * HEAD].astype(f32)
        nk_buf[:, h, :] = nk_ref[:, g * HEAD : (g + 1) * HEAD].astype(f32)
        nv_buf[:, h, :] = nv_ref[:, g * HEAD : (g + 1) * HEAD].astype(f32)
        x = column(flogit_ref[h : h + 1, :]) + fbias_ref[h]
        lf_buf[:, h, :] = jnp.broadcast_to(
            jnp.minimum(x, 0.0) - jnp.log1p(jnp.exp(-jnp.abs(x))), (tokens, HEAD)
        )
    head_row = lax.broadcasted_iota(jnp.int32, (heads, slots), 0)

    def owns(g):
        return (head_row >= g * grouping) & (head_row < (g + 1) * grouping)

    for n in range(tokens):
        if n % step == 0:
            cache[n // step].wait()
        len_buf[n] = jnp.full((heads, HEAD), len_ref[n], jnp.int32)
        every = lax.dot_general(
            q_buf[n].astype(bf16),
            kc[n].reshape(kv_local * slots, HEAD),
            (((1,), (1,)), ((), ())),
            preferred_element_type=f32,
        )
        picked = every[:, 0:slots]
        for g in range(1, kv_local):
            picked = jnp.where(owns(g), every[:, g * slots : (g + 1) * slots], picked)
        score_buf[n] = picked
    for load in loads[1:]:
        load.start()
    scale = 1.0 / math.sqrt(HEAD)
    own = jnp.sum(q_buf[...] * nk_buf[...], axis=2, keepdims=True) * scale
    cum = cum_ref[...]
    length = len_buf[:, :, 0:1]
    position = lax.broadcasted_iota(jnp.int32, (tokens, heads, slots), 2)
    latest = jnp.sum(jnp.where(position == length - 1, cum, 0.0), axis=2, keepdims=True)
    scores = score_buf[...] * scale + (latest + lf_buf[:, :, 0:1]) - cum
    scores = jnp.where(position < length, scores, -jnp.inf)
    highest = jnp.maximum(jnp.max(scores, axis=2, keepdims=True), own)
    past = jnp.exp(scores - highest)
    mine_own = jnp.exp(own - highest)
    totals = jnp.sum(past, axis=2, keepdims=True) + mine_own
    score_buf[...] = past / totals
    own_prob = (mine_own / totals).astype(bf16).astype(f32)
    for n in range(tokens):
        if n % step == 0:
            cache[CACHE_CHUNKS + n // step].wait()
        probs = score_buf[n]
        spread = jnp.concatenate(
            [jnp.where(owns(g), probs, 0.0) for g in range(kv_local)], axis=1
        ).astype(bf16)
        mix_buf[n] = jnp.dot(
            spread, vc[n].reshape(kv_local * slots, HEAD), preferred_element_type=f32
        )
    mix_buf[...] = mix_buf[...] + own_prob * nv_buf[...]
    for h in range(heads):
        att_buf[:, h * HEAD : (h + 1) * HEAD] = mix_buf[:, h, :].astype(bf16)

    loads[0].wait()
    head_part = jnp.dot(att_buf[...], ow[...], preferred_element_type=f32)
    pp_send[...] = head_part.astype(bf16)
    pl.semaphore_wait(barrier, ep_n - 1 + tp_n - 1)

    def remote(src, dst, ssem, rsem, to):
        return pltpu.make_async_remote_copy(
            src_ref=src,
            dst_ref=dst,
            send_sem=ssem,
            recv_sem=rsem,
            device_id=to,
            device_id_type=MESH,
        )

    sends = []
    pp = []
    for k in range(1, tp_n):
        c = remote(
            pp_send,
            pp_recv.at[k - 1],
            pp_ssem.at[k - 1],
            pp_rsem.at[k - 1],
            (ep, lax.rem(tp + k, tp_n)),
        )
        c.start()
        pp.append(c)
        sends.append(c)
    for c in pp:
        c.wait_recv()
    projected = head_part
    for k in range(tp_n - 1):
        projected = projected + pp_recv[k].astype(f32)
    state_full = resid_ref[...].astype(f32) + projected.astype(bf16).astype(f32)
    inverse = lax.rsqrt(jnp.mean(state_full * state_full, axis=1, keepdims=True) + EPSILON)
    scaled_full = state_full * gain_ref[...]
    gate = jax.nn.sigmoid(
        inverse * jnp.sum(scaled_full * mix_ref[...].astype(f32), axis=1, keepdims=True)
    )
    state_buf[...] = state_full
    norm_buf[...] = scaled_full * inverse
    cols = pl.ds(pl.multiple_of(tp * width, 128), width)
    gat[ep, :, 0:width] = norm_buf[:, cols].astype(bf16)
    lane = lax.broadcasted_iota(jnp.int32, (tokens, META), 1)
    named = [column(routes_ref[k : k + 1, :].astype(f32)) for k in range(TOP_K)]
    weighed = [column(rw_ref[k : k + 1, :]) for k in range(TOP_K)]
    meta = jnp.zeros((tokens, META), f32)
    for s in range(3):
        base = s * SEG
        value = jnp.where(lane == base, gate, 0.0)
        for k in range(TOP_K):
            value = value + jnp.where(
                (lane - base - 1).astype(f32) == named[k], weighed[k], 0.0
            )
        value = jnp.where((lane >= base) & (lane < base + SEG), value, 0.0)
        for cut in range(s):
            value = value - value.astype(bf16).astype(f32)
        meta = meta + value
    gat[ep, :, width : width + META] = meta.astype(bf16)

    c = remote(gat.at[ep], gat.at[ep], ag_psem.at[0], ag_rsem.at[ep], (partner, tp))
    c.start()
    sends.append(c)
    for i, j in enumerate(order):
        group = place(j)
        for b in range(cpg):
            if j == (0, 0) and b == 0:
                continue
            target = (group * cpg + lax.rem(inchip + b, cpg)) * 2 + core
            c = remote(
                gat.at[ep], gat.at[ep], ag_ssem.at[i * cpg + b], ag_rsem.at[ep], (target, tp)
            )
            c.start()
            sends.append(c)

    def arrive(src):
        remote(gat.at[src], gat.at[src], ag_psem.at[0], ag_rsem.at[src], (partner, tp)).wait_recv()

    def forward(i):
        j = order[i]
        group = place(j)
        for b in range(cpg):
            if j == (0, 0) and b == 0:
                continue
            src = (group * cpg + lax.rem(inchip + b, cpg)) * 2 + core
            arrive(src)
            c = remote(
                gat.at[src], gat.at[src], fwd_ssem.at[i * cpg + b], ag_rsem.at[src], (partner, tp)
            )
            c.start()
            sends.append(c)

    pcopies = {}
    hcopies = {}

    def stage_in(i):
        j = order[i]
        group = place(j)
        for b in range(cpg):
            arrive((group * cpg + lax.rem(inchip + b, cpg)) * 2 + 1 - core)
        x = gat[pl.ds(group * epg, epg), :, 0:width].reshape(rows, width)
        at = 0
        for n, w in enumerate((eg, eu, dg, du)):
            if i == 0:
                loads[1 + n].wait()
            if n < 2:
                size = w.shape[1]
                value = jnp.dot(x, w[...], preferred_element_type=f32)
            else:
                size = w.shape[0]
                value = lax.dot_general(
                    x, w[...], (((1,), (1,)), ((), ())), preferred_element_type=f32
                )
            pf[i, :, at : at + size] = value
            psend[i, :, at : at + size] = value.astype(bf16)
            at += size
        pcopies[i] = []
        for k in range(1, tp_n):
            to = lax.rem(tp + k, tp_n)
            c = remote(
                psend.at[i, pl.ds(pl.multiple_of(to * part, 16), part)],
                precv.at[i, k - 1],
                p_ssem.at[i, k - 1],
                p_rsem.at[i, k - 1],
                (ep, to),
            )
            c.start()
            sends.append(c)
            pcopies[i].append(c)

    def stage_mid(i):
        for c in pcopies[i]:
            c.wait_recv()
        mine = pl.ds(pl.multiple_of(tp * part, 16), part)

        def total(at, size):
            value = pf[i, mine, at : at + size]
            for k in range(tp_n - 1):
                value = value + precv[i, k, :, at : at + size].astype(f32)
            return value

        hid[i, mine, 0:span] = (jax.nn.silu(total(0, span)) * total(span, span)).astype(bf16)
        hid[i, mine, span : span + dspan] = (
            jax.nn.silu(total(2 * span, dspan)) * total(2 * span + dspan, dspan)
        ).astype(bf16)
        hcopies[i] = []
        for k in range(1, tp_n):
            to = lax.rem(tp + k, tp_n)
            c = remote(
                hid.at[i, mine],
                hid.at[i, mine],
                h_ssem.at[i, k - 1],
                h_rsem.at[i, k - 1],
                (ep, to),
            )
            c.start()
            sends.append(c)
            source = lax.rem(tp + tp_n - k, tp_n)
            theirs = pl.ds(pl.multiple_of(source * part, 16), part)
            hcopies[i].append(
                remote(
                    hid.at[i, theirs],
                    hid.at[i, theirs],
                    h_ssem.at[i, k - 1],
                    h_rsem.at[i, k - 1],
                    (ep, to),
                )
            )

    expert = ep // EXP_SPAN
    lanes = lax.broadcasted_iota(jnp.int32, (rows, META), 1)

    def stage_out(i):
        j = order[i]
        group = place(j)
        for c in hcopies[i]:
            c.wait_recv()
        if i == 0:
            loads[5].wait()
            loads[6].wait()
        info = gat[pl.ds(group * epg, epg), :, width : width + META].reshape(rows, META)
        info = info.astype(f32)
        gates = jnp.sum(
            jnp.where((lanes == 0) | (lanes == SEG) | (lanes == 2 * SEG), info, 0.0),
            axis=1,
            keepdims=True,
        )
        spot = lanes - expert - 1
        shares = jnp.sum(
            jnp.where((spot == 0) | (spot == SEG) | (spot == 2 * SEG), info, 0.0),
            axis=1,
            keepdims=True,
        )
        value = shares * jnp.dot(hid[i, :, 0:span], ed[...], preferred_element_type=f32)
        value = value + gates * jnp.dot(
            hid[i, :, span : span + dspan], dd[...], preferred_element_type=f32
        )
        rs_send[i] = value.astype(bf16).reshape(epg, tokens, width)
        member = lax.rem(ep, epg)
        for b in range(epg):
            slot = lax.rem(member + b, epg)
            if j == (0, 0) and b == 0:
                rs_recv[ep] = rs_send[i, slot]
                continue
            c = remote(
                rs_send.at[i, slot],
                rs_recv.at[ep],
                rs_ssem.at[i * epg + b],
                rs_rsem.at[ep],
                (group * epg + slot, tp),
            )
            c.start()
            sends.append(c)

    for i in range(min(AHEAD, groups)):
        forward(i)
    for i in range(groups + OUT_LAG):
        if i < groups:
            stage_in(i)
        if i + AHEAD < groups:
            forward(i + AHEAD)
        if 0 <= i - MID_LAG < groups:
            stage_mid(i - MID_LAG)
        if i >= OUT_LAG:
            stage_out(i - OUT_LAG)

    for k in range(1, ep_n):
        src = lax.rem(ep + k, ep_n)
        remote(
            rs_recv.at[src], rs_recv.at[src], rs_ssem.at[0], rs_rsem.at[src], (partner, tp)
        ).wait_recv()
    result = state_buf[:, cols] + jnp.sum(rs_recv[...].astype(f32), axis=0)
    out_ref[...] = result
    for c in sends:
        c.wait_send()


def layer_call(
    q, nk, nv, cum, flogit, fbias, lengths, resid, gain, mix, routes, route_weight, kc, vc, ow, eg,
    eu, ed, dg, du, dd,
):
    ep_n, tp_n = lax.axis_size("ep"), lax.axis_size("tp")
    groups = GROUPS if (ep_n // 2) % GROUPS == 0 else 1
    order = ORDER if groups == GROUPS else ((0, 0),)
    tokens, full = resid.shape
    width = full // tp_n
    epg = ep_n // groups
    rows = epg * tokens
    part = rows // tp_n
    span, dspan = eg.shape[2], dg.shape[0]
    hidden = span + dspan
    assert ep_n // EXP_SPAN + 1 <= SEG
    f32, bf16 = jnp.float32, jnp.bfloat16
    heads = cum.shape[1]
    smem = pl.BlockSpec(memory_space=pltpu.SMEM)
    vmem = pl.BlockSpec(memory_space=pltpu.VMEM)
    hbm = pl.BlockSpec(memory_space=pl.ANY)
    dma = pltpu.SemaphoreType.DMA
    peers = max(tp_n - 1, 1)
    return pl.pallas_call(
        functools.partial(layer_kernel, (ep_n, tp_n, groups, order)),
        out_shape=jax.ShapeDtypeStruct((tokens, width), f32),
        in_specs=[vmem] * 5 + [smem] * 2 + [vmem] * 5 + [hbm] * 9,
        out_specs=vmem,
        scratch_shapes=[
            pltpu.VMEM(kc.shape, bf16),
            pltpu.VMEM(vc.shape, bf16),
            pltpu.VMEM((tokens, heads, HEAD), f32),
            pltpu.VMEM((tokens, heads, HEAD), f32),
            pltpu.VMEM((tokens, heads, HEAD), f32),
            pltpu.VMEM((tokens, heads, HEAD), f32),
            pltpu.VMEM((tokens, heads, HEAD), jnp.int32),
            pltpu.VMEM(cum.shape, f32),
            pltpu.VMEM((tokens, heads, HEAD), f32),
            pltpu.VMEM((tokens, heads * HEAD), bf16),
            pltpu.VMEM(ow.shape, bf16),
            pltpu.VMEM(eg.shape[1:], bf16),
            pltpu.VMEM(eu.shape[1:], bf16),
            pltpu.VMEM(ed.shape[1:], bf16),
            pltpu.VMEM(dg.shape, bf16),
            pltpu.VMEM(du.shape, bf16),
            pltpu.VMEM(dd.shape, bf16),
            pltpu.VMEM((tokens, full), bf16),
            pltpu.VMEM((peers, tokens, full), bf16),
            pltpu.VMEM((tokens, full), f32),
            pltpu.VMEM((tokens, full), f32),
            pltpu.VMEM((ep_n, tokens, width + META), bf16),
            pltpu.VMEM((groups, rows, 2 * hidden), f32),
            pltpu.VMEM((groups, rows, 2 * hidden), bf16),
            pltpu.VMEM((groups, peers, part, 2 * hidden), bf16),
            pltpu.VMEM((groups, rows, hidden), bf16),
            pltpu.VMEM((groups, epg, tokens, width), bf16),
            pltpu.VMEM((ep_n, tokens, width), bf16),
            dma((7,)),
            dma((2, CACHE_CHUNKS)),
            dma((peers,)),
            dma((peers,)),
            dma((ep_n // 2,)),
            dma((1,)),
            dma((ep_n // 2,)),
            dma((ep_n,)),
            dma((groups, peers)),
            dma((groups, peers)),
            dma((groups, peers)),
            dma((groups, peers)),
            dma((ep_n,)),
            dma((ep_n,)),
        ],
        compiler_params=pltpu.CompilerParams(
            collective_id=0, has_side_effects=True, vmem_limit_bytes=VMEM_LIMIT
        ),
        name="layer",
    )(
        q, nk, nv, cum, flogit, fbias, lengths, resid, gain, mix, routes, route_weight, kc, vc, ow,
        eg, eu, ed, dg, du, dd,
    )


def body(
    resid,
    queries,
    new_keys,
    new_values,
    key_cache,
    value_cache,
    cum_gate,
    forget_logit,
    forget_bias,
    lengths,
    out_weight,
    norm_gain,
    mix_vector,
    routes,
    route_weight,
    expert_gate,
    expert_up,
    expert_down,
    dense_gate,
    dense_up,
    dense_down,
):
    result = layer_call(
        queries,
        new_keys,
        new_values,
        cum_gate,
        forget_logit.T,
        forget_bias,
        lengths,
        resid,
        norm_gain.reshape(1, -1),
        mix_vector.astype(jnp.float32).reshape(1, -1),
        routes.T,
        route_weight.T,
        key_cache,
        value_cache,
        out_weight,
        expert_gate,
        expert_up,
        expert_down,
        dense_gate.T,
        dense_up.T,
        dense_down,
    )
    return result.astype(jnp.bfloat16)


def solution(mesh):
    placed = (
        P("ep", None),
        P("ep", "tp"),
        P("ep", "tp"),
        P("ep", "tp"),
        P("ep", "tp", None, None),
        P("ep", "tp", None, None),
        P("ep", "tp", None),
        P("ep", "tp"),
        P("tp"),
        P("ep"),
        P("tp", None),
        P(),
        P(),
        P("ep", None),
        P("ep", None),
        P("ep", "tp", None),
        P("ep", "tp", None),
        P("ep", None, "tp"),
        P("tp", "ep"),
        P("tp", "ep"),
        P("ep", "tp"),
    )
    return jax.shard_map(body, mesh=mesh, in_specs=placed, out_specs=P("ep", "tp"), check_vma=False)
```

profile of v0, /device:TPU:0, one launch (start us, length us, event | category | flops | bytes accessed | tf_op | source)
XLA Modules:
  0.0 44.8 jit_solution(11048070016120077041)
XLA Ops:
  0.0 1.3 %reshape.11 = f32[2048]{0:T(1024)} convert(bf16[2048]{0:T(1024)(128)(2,1)} %param.33) | non-fusion elementwise | flops 2048 | bytes 12288 | tf_op jit(solution)/shard_map/reshape | solution.py:578
  1.3 42.1 %layer.1 = f32[16,1024]{1,0:T(8,128)} custom-call(bf16[16,512]{1,0:T(8,128)(2,1)} %q_ref.1, bf16[16,256]{1,0:T(8,128)(2,1)} %nk_ref.1, bf16[16,256]{1,0:T(8,128)(2,1)} %nv_ref.1, f32[16,4,256]{2,1,0:T(4,128)} %cum_ref.1, f32[4,16]{1,0:T(4,128)} %bitcast.11, f32[4]{0:T(128)} %fbias_ref.1, s32[16]{0:T(128)} %len_ref.1, bf16[16,2048]{1,0:T(8,128)(2,1)} %resid_ref.1, ...), custom_call_target="tpu_custom_call" | custom-call | tf_op jit(solution)/shard_map/layer/pallas_call | solution.py:486
  43.4 1.5 %convert_element_type.4 = bf16[16,1024]{1,0:T(8,128)(2,1)} convert(f32[16,1024]{1,0:T(8,128)} %layer.1) | non-fusion elementwise | flops 16384 | bytes 98304 | tf_op jit(solution)/shard_map/convert_element_type | solution.py:591
where the time goes:
time: 45.1 us; the launch traced here: 44.8 us
  Pallas kernels  42.1 us (93%)
  other arithmetic  2.74 us (6%)
    pallas_call x1, Pallas kernels, layer_call(): pl.pallas_call(functools.partial(layer_kernel, (ep_n, tp_n, groups, order...  42.1 us
    convert_element_type x1, other arithmetic, body(): return result.astype(jnp.bfloat16)  1.46 us
    reshape x1, other arithmetic, body(): mix_vector.astype(jnp.float32).reshape(1, -1)  1.29 us

commit v1 on v0

--- a/solution.py
+++ b/solution.py
@@ -18,12 +18,42 @@
 META = 128
 SEG = 42
 GROUPS = 8
-INNER = 2
-ORDER = ((0, 0), (0, 1), (2, 0), (2, 1), (1, 0), (1, 1), (3, 0), (3, 1))
+ORDER = (0, 1, 4, 5, 6, 7, 2, 3)
 CACHE_CHUNKS = 4
-AHEAD = 3
-MID_LAG = 2
-OUT_LAG = 4
+STEPS = (
+    ("fwd", 0),
+    ("in", 0),
+    ("fwd", 1),
+    ("fwd", 2),
+    ("in", 1),
+    ("fwd", 3),
+    ("in", 2),
+    ("mid", 0),
+    ("fwd", 4),
+    ("in", 3),
+    ("mid", 1),
+    ("fwd", 5),
+    ("in", 4),
+    ("mid", 2),
+    ("fwd", 6),
+    ("in", 5),
+    ("mid", 3),
+    ("out", 1),
+    ("fwd", 7),
+    ("in", 6),
+    ("mid", 4),
+    ("out", 2),
+    ("in", 7),
+    ("mid", 5),
+    ("out", 3),
+    ("mid", 6),
+    ("out", 4),
+    ("mid", 7),
+    ("out", 5),
+    ("out", 6),
+    ("out", 7),
+    ("out", 0),
+)
 VMEM_LIMIT = 60 * 1024 * 1024
 
 
@@ -111,13 +141,9 @@
     partner = chip * 2 + 1 - core
     mygroup = chip // cpg
     inchip = lax.rem(chip, cpg)
-    inner = max(1, min(INNER, groups))
-    outer = groups // inner
 
     def place(j):
-        high = lax.rem(mygroup // inner + j[0], outer)
-        return high * inner + lax.rem(lax.rem(mygroup, inner) + j[1], inner)
-
+        return mygroup ^ j
 
     kv_local = kc.shape[1]
     heads = q_buf.shape[1]
@@ -260,9 +286,11 @@
     state_full = resid_ref[...].astype(f32) + projected.astype(bf16).astype(f32)
     inverse = lax.rsqrt(jnp.mean(state_full * state_full, axis=1, keepdims=True) + EPSILON)
     scaled_full = state_full * gain_ref[...]
-    gate = jax.nn.sigmoid(
-        inverse * jnp.sum(scaled_full * mix_ref[...].astype(f32), axis=1, keepdims=True)
-    )
+    mix = mix_ref[...].astype(f32)
+    mixed = jnp.zeros((tokens, HEAD), f32)
+    for n in range(mix.shape[0]):
+        mixed = mixed + scaled_full[:, n * HEAD : (n + 1) * HEAD] * mix[n : n + 1, :]
+    gate = jax.nn.sigmoid(inverse * jnp.sum(mixed, axis=1, keepdims=True))
     state_buf[...] = state_full
     norm_buf[...] = scaled_full * inverse
     cols = pl.ds(pl.multiple_of(tp * width, 128), width)
@@ -290,7 +318,7 @@
     for i, j in enumerate(order):
         group = place(j)
         for b in range(cpg):
-            if j == (0, 0) and b == 0:
+            if j == 0 and b == 0:
                 continue
             target = (group * cpg + lax.rem(inchip + b, cpg)) * 2 + core
             c = remote(
@@ -306,7 +334,7 @@
         j = order[i]
         group = place(j)
         for b in range(cpg):
-            if j == (0, 0) and b == 0:
+            if j == 0 and b == 0:
                 continue
             src = (group * cpg + lax.rem(inchip + b, cpg)) * 2 + core
             arrive(src)
@@ -318,6 +346,7 @@
 
     pcopies = {}
     hcopies = {}
+    late = [loads[5], loads[6]]
 
     def stage_in(i):
         j = order[i]
@@ -401,9 +430,8 @@
         group = place(j)
         for c in hcopies[i]:
             c.wait_recv()
-        if i == 0:
-            loads[5].wait()
-            loads[6].wait()
+        while late:
+            late.pop().wait()
         info = gat[pl.ds(group * epg, epg), :, width : width + META].reshape(rows, META)
         info = info.astype(f32)
         gates = jnp.sum(
@@ -425,7 +453,7 @@
         member = lax.rem(ep, epg)
         for b in range(epg):
             slot = lax.rem(member + b, epg)
-            if j == (0, 0) and b == 0:
+            if j == 0 and b == 0:
                 rs_recv[ep] = rs_send[i, slot]
                 continue
             c = remote(
@@ -438,17 +466,12 @@
             c.start()
             sends.append(c)
 
-    for i in range(min(AHEAD, groups)):
-        forward(i)
-    for i in range(groups + OUT_LAG):
-        if i < groups:
-            stage_in(i)
-        if i + AHEAD < groups:
-            forward(i + AHEAD)
-        if 0 <= i - MID_LAG < groups:
-            stage_mid(i - MID_LAG)
-        if i >= OUT_LAG:
-            stage_out(i - OUT_LAG)
+    stages = {"in": stage_in, "fwd": forward, "mid": stage_mid, "out": stage_out}
+    steps = STEPS
+    if groups == 1:
+        steps = (("fwd", 0), ("in", 0), ("mid", 0), ("out", 0))
+    for stage, i in steps:
+        stages[stage](i)
 
     for k in range(1, ep_n):
         src = lax.rem(ep + k, ep_n)
@@ -456,7 +479,7 @@
             rs_recv.at[src], rs_recv.at[src], rs_ssem.at[0], rs_rsem.at[src], (partner, tp)
         ).wait_recv()
     result = state_buf[:, cols] + jnp.sum(rs_recv[...].astype(f32), axis=0)
-    out_ref[...] = result
+    out_ref[...] = result.astype(bf16)
     for c in sends:
         c.wait_send()
 
@@ -467,7 +490,7 @@
 ):
     ep_n, tp_n = lax.axis_size("ep"), lax.axis_size("tp")
     groups = GROUPS if (ep_n // 2) % GROUPS == 0 else 1
-    order = ORDER if groups == GROUPS else ((0, 0),)
+    order = ORDER if groups == GROUPS else (0,)
     tokens, full = resid.shape
     width = full // tp_n
     epg = ep_n // groups
@@ -485,7 +508,7 @@
     peers = max(tp_n - 1, 1)
     return pl.pallas_call(
         functools.partial(layer_kernel, (ep_n, tp_n, groups, order)),
-        out_shape=jax.ShapeDtypeStruct((tokens, width), f32),
+        out_shape=pltpu.VMEM((tokens, width), bf16),
         in_specs=[vmem] * 5 + [smem] * 2 + [vmem] * 5 + [hbm] * 9,
         out_specs=vmem,
         scratch_shapes=[
@@ -575,7 +598,7 @@
         lengths,
         resid,
         norm_gain.reshape(1, -1),
-        mix_vector.astype(jnp.float32).reshape(1, -1),
+        mix_vector.reshape(-1, HEAD),
         routes.T,
         route_weight.T,
         key_cache,
@@ -588,7 +611,7 @@
         dense_up.T,
         dense_down,
     )
-    return result.astype(jnp.bfloat16)
+    return result
 
 
 def solution(mesh):

time: 45.1 us -> 41.5 us (0.920)
  other arithmetic: 2.74 us -> 0 us
  Pallas kernels: 42.1 us -> 40.7 us
  local copies, waits for them, and re-layouts: 0 us -> 0.62 us
    convert_element_type x1 -> x0, other arithmetic: 1.46 us -> none  [body(): return result.astype(jnp.bfloat16)]
    pallas_call x1, Pallas kernels: 42.1 us -> 40.7 us  [layer_call(): pl.pallas_call(functools.partial(layer_kernel, (ep_n, tp_n, groups, order...]
    reshape x1 -> x0, other arithmetic: 1.29 us -> none  [body(): mix_vector.astype(jnp.float32).reshape(1, -1)]
    unnamed x0 -> x1, local copies, waits for them, and re-layouts: none -> 0.62 us
where the time goes in v1:
time: 41.5 us; the launch traced here: 41.4 us
  Pallas kernels  40.7 us (98%)
  local copies, waits for them, and re-layouts  0.62 us (1%)
    pallas_call x1, Pallas kernels, layer_call(): pl.pallas_call(functools.partial(layer_kernel, (ep_n, tp_n, groups, order...  40.7 us

profile of v1, /device:TPU:0, one launch (start us, length us, event | category | flops | bytes accessed | tf_op | source)
XLA Modules:
  0.0 41.4 jit_solution(12894448809274610062)
XLA Ops:
  0.0 40.7 %layer.1 = bf16[16,1024]{1,0:T(8,128)(2,1)S(1)} custom-call(bf16[16,512]{1,0:T(8,128)(2,1)} %q_ref.1, bf16[16,256]{1,0:T(8,128)(2,1)} %nk_ref.1, bf16[16,256]{1,0:T(8,128)(2,1)} %nv_ref.1, f32[16,4,256]{2,1,0:T(4,128)} %cum_ref.1, f32[4,16]{1,0:T(4,128)} %bitcast.11, f32[4]{0:T(128)} %fbias_ref.1, s32[16]{0:T(128)} %len_ref.1, bf16[16,2048]{1,0:T(8,128)(2,1)} %resid_ref.1, ...), custom_call_target="tpu_custom_call" | custom-call | tf_op jit(solution)/shard_map/layer/pallas_call | solution.py:509
  40.7 0.6 %copy.23 = bf16[16,1024]{1,0:T(8,128)(2,1)} copy(bf16[16,1024]{1,0:T(8,128)(2,1)S(1)} %layer.1) | data formatting | bytes 65536

commit v2 on v1

v2 whole, which is shorter than its diff:
```python
import functools
import math

import jax
import jax.numpy as jnp
from jax import lax
from jax.experimental import pallas as pl
from jax.experimental.pallas import tpu as pltpu
from jax.sharding import PartitionSpec as P

HEAD = 128
TOP_K = 2
EXP_SPAN = 4


EPSILON = 1e-06
MESH = pl.DeviceIdType.MESH
META = 128
SEG = 42
PLANES = 4
FAR = (1, 2, 3)
STEPS = (
    ("fwd", 0),
    ("in", 0),
    ("in", 1),
    ("fwd", 2),
    ("in", 2),
    ("fwd", 3),
    ("mid", 1),
    ("in", 3),
    ("fwd", 4),
    ("mid", 2),
    ("in", 4),
    ("mid", 0),
    ("out", 1),
    ("red", 1),
    ("mid", 3),
    ("out", 0),
    ("red", 0),
    ("out", 2),
    ("mid", 4),
    ("red", 2),
    ("out", 3),
    ("red", 3),
    ("out", 4),
    ("red", 4),
)
CACHE_CHUNKS = 4
VMEM_LIMIT = 60 * 1024 * 1024


def layer_kernel(
    dims,
    q_hbm,
    nk_hbm,
    nv_hbm,
    cum_hbm,
    flogit_hbm,
    fbias_hbm,
    len_hbm,
    resid_hbm,
    gain_hbm,
    mix_hbm,
    routes_hbm,
    rw_hbm,
    kc_hbm,
    vc_hbm,
    ow_hbm,
    eg_hbm,
    eu_hbm,
    ed_hbm,
    dg_hbm,
    du_hbm,
    dd_hbm,
    out_ref,
    q_ref,
    nk_ref,
    nv_ref,
    cum_ref,
    flogit_ref,
    fbias_ref,
    len_ref,
    resid_ref,
    gain_ref,
    mix_ref,
    routes_ref,
    rw_ref,
    kc,
    vc,
    q_buf,
    nk_buf,
    nv_buf,
    lf_buf,
    len_buf,
    add_buf,
    score_buf,
    mix_buf,
    att_buf,
    ow,
    wgu,
    wd,
    dgu,
    pp_send,
    pp_recv,
    state_buf,
    norm_buf,
    gat,
    pf,
    psend,
    precv,
    aff,
    asend,
    arecv,
    hid,
    outs,
    cs_send,
    cs_recv,
    rs_send,
    rs_recv,
    small_sem,
    load_sem,
    cache_sem,
    pp_ssem,
    pp_rsem,
    ag_ssem,
    ag_psem,
    ag_rsem,
    p_ssem,
    p_rsem,
    h_ssem,
    h_rsem,
    c_ssem,
    c_rsem,
    rs_ssem,
    rs_rsem,
):
    ep_n, tp_n, sets = dims
    ep = lax.axis_index("ep")
    tp = lax.axis_index("tp")
    f32, bf16 = jnp.float32, jnp.bfloat16
    tokens, width = out_ref.shape
    span = eg_hbm.shape[2]
    dspan = dg_hbm.shape[0]
    hidden = span + dspan
    chips = ep_n // 2
    chip = ep // 2
    core = lax.rem(ep, 2)
    partner = chip * 2 + 1 - core
    sizes = [2 * count * tokens for count, where, direct, whole in sets]
    firsts = [sum(sizes[:i]) for i in range(len(sets))]

    kv_local = kc.shape[1]
    heads = q_buf.shape[1]
    slots = kc.shape[2]
    grouping = heads // kv_local
    step = tokens // CACHE_CHUNKS
    cache = []
    for side, (src, dst) in enumerate(((kc_hbm, kc), (vc_hbm, vc))):
        for n in range(CACHE_CHUNKS):
            some = pl.ds(n * step, step)
            cache.append(
                pltpu.make_async_copy(src.at[some], dst.at[some], cache_sem.at[side, n])
            )
    smalls = [
        pltpu.make_async_copy(src, dst, small_sem.at[i])
        for i, (src, dst) in enumerate(
            [
                (q_hbm, q_ref),
                (nk_hbm, nk_ref),
                (nv_hbm, nv_ref),
                (flogit_hbm, flogit_ref),
                (fbias_hbm, fbias_ref),
                (len_hbm, len_ref),
                (cum_hbm, cum_ref),
                (resid_hbm, resid_ref),
                (gain_hbm, gain_ref),
                (mix_hbm, mix_ref),
                (routes_hbm, routes_ref),
                (rw_hbm, rw_ref),
            ]
        )
    ]
    smalls[0].start()
    cache[0].start()
    for load in smalls[1:7]:
        load.start()
    for load in cache[1:]:
        load.start()
    loads = [
        pltpu.make_async_copy(src, dst, load_sem.at[i])
        for i, (src, dst) in enumerate(
            [
                (ow_hbm, ow),
                (dg_hbm, dgu.at[0:dspan]),
                (du_hbm, dgu.at[dspan : 2 * dspan]),
                (eg_hbm.at[0], wgu.at[:, 0:span]),
                (eu_hbm.at[0], wgu.at[:, span : 2 * span]),
                (ed_hbm.at[0], wd.at[0:span]),
                (dd_hbm, wd.at[span:hidden]),
            ]
        )
    ]
    loads[0].start()
    for load in smalls[7:]:
        load.start()

    barrier = pltpu.get_barrier_semaphore()
    for k in range(1, ep_n):
        pl.semaphore_signal(
            barrier, inc=1, device_id=(lax.rem(ep + k, ep_n), tp), device_id_type=MESH
        )
    for k in range(1, tp_n):
        pl.semaphore_signal(
            barrier, inc=1, device_id=(ep, lax.rem(tp + k, tp_n)), device_id_type=MESH
        )

    eye = lax.broadcasted_iota(jnp.int32, (tokens, tokens), 0) == lax.broadcasted_iota(
        jnp.int32, (tokens, tokens), 1
    )

    def column(row):
        return jnp.sum(jnp.where(eye, row, 0.0), axis=1, keepdims=True)

    q_buf[...] = jnp.zeros_like(q_buf)
    for load in smalls[0:6]:
        load.wait()
    for h in range(heads):
        g = h // grouping
        one = slice(g * HEAD, (g + 1) * HEAD)
        q_buf[:, h, one] = q_ref[:, h * HEAD : (h + 1) * HEAD].astype(f32)
        nk_buf[:, h, :] = nk_ref[...].astype(f32)
        nv_buf[:, h, :] = nv_ref[:, one].astype(f32)
        x = column(flogit_ref[h : h + 1, :]) + fbias_ref[h]
        lf_buf[:, h, :] = jnp.broadcast_to(
            jnp.minimum(x, 0.0) - jnp.log1p(jnp.exp(-jnp.abs(x))), (tokens, HEAD)
        )
    head_row = lax.broadcasted_iota(jnp.int32, (heads, HEAD), 0)
    for n in range(tokens):
        len_buf[n] = jnp.full((heads, HEAD), len_ref[n], jnp.int32)

    def beside(ref, n):
        return jnp.concatenate([ref[n, g] for g in range(kv_local)], axis=1)

    scale = 1.0 / math.sqrt(HEAD)
    own = jnp.sum(q_buf[...] * nk_buf[...], axis=2, keepdims=True) * scale
    smalls[6].wait()
    cum = cum_ref[...]
    length = len_buf[:, :, 0:1]
    position = lax.broadcasted_iota(jnp.int32, (tokens, heads, slots), 2)
    latest = jnp.sum(jnp.where(position == length - 1, cum, 0.0), axis=2, keepdims=True)
    add_buf[...] = jnp.where(
        position < length, (latest + lf_buf[:, :, 0:1]) - cum, -jnp.inf
    )
    for n in range(tokens):
        if n % step == 0:
            cache[n // step].wait()
        score_buf[n] = lax.dot_general(
            q_buf[n].astype(bf16),
            beside(kc, n),
            (((1,), (1,)), ((), ())),
            preferred_element_type=f32,
        )
    for load in loads[1:]:
        load.start()
    scores = score_buf[...] * scale + add_buf[...]
    highest = jnp.maximum(jnp.max(scores, axis=2, keepdims=True), own)
    past = jnp.exp(scores - highest)
    mine_own = jnp.exp(own - highest)
    totals = jnp.sum(past, axis=2, keepdims=True) + mine_own
    score_buf[...] = past / totals
    own_prob = (mine_own / totals).astype(bf16).astype(f32)
    for n in range(tokens):
        if n % step == 0:
            cache[CACHE_CHUNKS + n // step].wait()
        both = jnp.dot(score_buf[n].astype(bf16), beside(vc, n), preferred_element_type=f32)
        taken = both[:, 0:HEAD]
        for g in range(1, kv_local):
            taken = jnp.where(
                head_row >= g * grouping, both[:, g * HEAD : (g + 1) * HEAD], taken
            )
        mix_buf[n] = taken
    mix_buf[...] = mix_buf[...] + own_prob * nv_buf[...]
    for h in range(heads):
        att_buf[:, h * HEAD : (h + 1) * HEAD] = mix_buf[:, h, :].astype(bf16)

    loads[0].wait()
    head_part = jnp.dot(att_buf[...], ow[...], preferred_element_type=f32)
    pp_send[...] = head_part.astype(bf16)
    pl.semaphore_wait(barrier, ep_n - 1 + tp_n - 1)

    def remote(src, dst, ssem, rsem, to):
        return pltpu.make_async_remote_copy(
            src_ref=src,
            dst_ref=dst,
            send_sem=ssem,
            recv_sem=rsem,
            device_id=to,
            device_id_type=MESH,
        )

    sends = []
    pp = []
    for k in range(1, tp_n):
        c = remote(
            pp_send,
            pp_recv.at[k - 1],
            pp_ssem.at[k - 1],
            pp_rsem.at[k - 1],
            (ep, lax.rem(tp + k, tp_n)),
        )
        c.start()
        pp.append(c)
        sends.append(c)
    for load in smalls[7:]:
        load.wait()
    loads[1].wait()
    loads[2].wait()
    wgu[:, 2 * span : 2 * hidden] = dgu[...].T
    for c in pp:
        c.wait_recv()
    projected = head_part
    for k in range(tp_n - 1):
        projected = projected + pp_recv[k].astype(f32)
    state_full = resid_ref[...].astype(f32) + projected.astype(bf16).astype(f32)
    inverse = lax.rsqrt(jnp.mean(state_full * state_full, axis=1, keepdims=True) + EPSILON)
    scaled_full = state_full * gain_ref[...]
    mix = mix_ref[...].astype(f32)
    mixed = jnp.zeros((tokens, HEAD), f32)
    for n in range(mix.shape[0]):
        mixed = mixed + scaled_full[:, n * HEAD : (n + 1) * HEAD] * mix[n : n + 1, :]
    gate = jax.nn.sigmoid(inverse * jnp.sum(mixed, axis=1, keepdims=True))
    state_buf[...] = state_full
    norm_buf[...] = scaled_full * inverse
    cols = pl.ds(pl.multiple_of(tp * width, 128), width)
    gat[core, chip, :, 0:width] = norm_buf[:, cols].astype(bf16)
    lane = lax.broadcasted_iota(jnp.int32, (tokens, META), 1)
    named = [column(routes_ref[k : k + 1, :].astype(f32)) for k in range(TOP_K)]
    weighed = [column(rw_ref[k : k + 1, :]) for k in range(TOP_K)]
    meta = jnp.zeros((tokens, META), f32)
    for s in range(3):
        base = s * SEG
        value = jnp.where(lane == base, gate, 0.0)
        for k in range(TOP_K):
            value = value + jnp.where(
                (lane - base - 1).astype(f32) == named[k], weighed[k], 0.0
            )
        value = jnp.where((lane >= base) & (lane < base + SEG), value, 0.0)
        for cut in range(s):
            value = value - value.astype(bf16).astype(f32)
        meta = meta + value
    gat[core, chip, :, width : width + META] = meta.astype(bf16)

    def put(src, dst, ssem, rsem, to):
        c = remote(src, dst, ssem, rsem, to)
        c.start()
        sends.append(c)
        return c

    block = gat.at[core, chip]
    put(block, block, ag_psem.at[0], ag_rsem.at[core, chip], (partner, tp))

    def others(i):
        count, where, direct, whole = sets[i]
        first = where(chip)
        for b in range(count):
            if whole and b == 0:
                continue
            yield first + lax.rem(chip + b, count) if count > 1 else first

    number = [0]

    def spot():
        number[0] += 1
        return number[0] - 1

    for i in range(len(sets)):
        for there in others(i):
            put(block, block, ag_ssem.at[spot()], ag_rsem.at[core, chip], (there * 2 + core, tp))
            if sets[i][2]:
                put(
                    block,
                    block,
                    ag_ssem.at[spot()],
                    ag_rsem.at[core, chip],
                    (there * 2 + 1 - core, tp),
                )

    def arrive(side, there):
        came = gat.at[side, there]
        remote(came, came, ag_psem.at[0], ag_rsem.at[side, there], (partner, tp)).wait_recv()

    def forward(i):
        for there in others(i):
            arrive(core, there)
            came = gat.at[core, there]
            if not sets[i][2]:
                put(came, came, ag_ssem.at[spot()], ag_rsem.at[core, there], (partner, tp))

    pcopies = {}
    hcopies = {}
    early = loads[3:5]
    late = loads[5:7]

    def piece(i, k):
        count, where, direct, whole = sets[i]
        share = 2 * count // tp_n
        at = k * share
        return gat.at[at // count, pl.ds(where(chip) + lax.rem(at, count), share)]

    def everything(i):
        count, where, direct, whole = sets[i]
        return [gat.at[side, pl.ds(where(chip), count)] for side in range(2)]

    def stage_in(i):
        count, where, direct, whole = sets[i]
        if direct:
            forward(i)
        if whole:
            arrive(1 - core, chip)
        for there in others(i):
            arrive(1 - core, there)
        while early:
            early.pop().wait()
        pcopies[i] = []
        if whole:
            pieces = everything(i)
        else:
            pieces = [piece(i, lax.rem(tp + k, tp_n)) for k in range(tp_n)]
        x = jnp.concatenate(
            [one[:, :, 0:width].reshape(sizes[i] // len(pieces), width) for one in pieces], axis=0
        )
        value = jnp.dot(x, wgu[...], preferred_element_type=f32)
        if whole:
            aff[...] = value
            asend[...] = value.astype(bf16)
        else:
            part = sizes[i] // tp_n
            at = pl.ds(firsts[i] // tp_n, part)
            pf[at] = value[0:part]
        for k in range(1, tp_n):
            if whole:
                src, dst = asend, arecv.at[k - 1]
            else:
                psend[k - 1, at] = value[k * part : (k + 1) * part].astype(bf16)
                src, dst = psend.at[k - 1, at], precv.at[k - 1, at]
            pcopies[i].append(
                put(
                    src,
                    dst,
                    p_ssem.at[i, k - 1],
                    p_rsem.at[i, k - 1],
                    (ep, lax.rem(tp + k, tp_n)),
                )
            )

    expert = ep // EXP_SPAN

    def stage_mid(i):
        for c in pcopies[i]:
            c.wait_recv()
        whole = sets[i][3]
        hcopies[i] = []
        if whole:
            part, pieces = sizes[i], everything(i)
            own, other, at = aff, arecv, pl.ds(0, part)
        else:
            part, pieces = sizes[i] // tp_n, [piece(i, tp)]
            own, other, at = pf, precv, pl.ds(firsts[i] // tp_n, part)

        def total(low, size):
            value = own[at, low : low + size]
            for k in range(tp_n - 1):
                value = value + other[k, at, low : low + size].astype(f32)
            return value

        lanes = lax.broadcasted_iota(jnp.int32, (part, META), 1)
        info = jnp.concatenate(
            [
                one[:, :, width : width + META].reshape(part // len(pieces), META)
                for one in pieces
            ],
            axis=0,
        ).astype(f32)

        def picked(lane):
            spot = lanes - lane
            return jnp.sum(
                jnp.where((spot == 0) | (spot == SEG) | (spot == 2 * SEG), info, 0.0),
                axis=1,
                keepdims=True,
            )

        routed = picked(expert + 1) * jax.nn.silu(total(0, span)) * total(span, span)
        dense = picked(0) * jax.nn.silu(total(2 * span, dspan)) * total(2 * span + dspan, dspan)
        if whole:
            mine = pl.ds(firsts[i], part)
        else:
            mine = pl.ds(pl.multiple_of(firsts[i] + tp * part, 16), part)
        hid[mine, 0:span] = routed.astype(bf16)
        hid[mine, span:hidden] = dense.astype(bf16)
        if whole:
            return
        for k in range(1, tp_n):
            to = lax.rem(tp + k, tp_n)
            put(hid.at[mine], hid.at[mine], h_ssem.at[i, k - 1], h_rsem.at[i, k - 1], (ep, to))
            source = lax.rem(tp + tp_n - k, tp_n)
            theirs = pl.ds(pl.multiple_of(firsts[i] + source * part, 16), part)
            hcopies[i].append(
                remote(
                    hid.at[theirs],
                    hid.at[theirs],
                    h_ssem.at[i, k - 1],
                    h_rsem.at[i, k - 1],
                    (ep, to),
                )
            )

    ccopies = {}

    def stage_out(i):
        for c in hcopies[i]:
            c.wait_recv()
        while late:
            late.pop().wait()
        value = jnp.dot(
            hid[firsts[i] : firsts[i] + sizes[i]], wd[...], preferred_element_type=f32
        )
        half = sizes[i] // 2
        at = pl.ds(firsts[i] // 2, half)
        outs[0, at] = value[0:half]
        outs[1, at] = value[half : 2 * half]
        cs_send[at] = outs[1 - core, at].astype(bf16)
        ccopies[i] = put(
            cs_send.at[at], cs_recv.at[at], c_ssem.at[i], c_rsem.at[i], (partner, tp)
        )

    def stage_red(i):
        count, where, direct, whole = sets[i]
        ccopies[i].wait_recv()
        at = pl.ds(firsts[i] // 2, sizes[i] // 2)
        value = outs[core, at] + cs_recv[at].astype(f32)
        first = firsts[i] // 2 // tokens
        rs_send[pl.ds(first, count)] = value.astype(bf16).reshape(count, tokens, width)
        for b in range(count):
            slot = lax.rem(chip + b, count)
            if whole and b == 0:
                rs_recv[chip] = rs_send[first + slot]
                continue
            put(
                rs_send.at[first + slot],
                rs_recv.at[chip],
                rs_ssem.at[first + b],
                rs_rsem.at[chip],
                ((where(chip) + slot) * 2 + core, tp),
            )

    stages = {
        "in": stage_in,
        "fwd": forward,
        "mid": stage_mid,
        "out": stage_out,
        "red": stage_red,
    }
    steps = STEPS
    if len(sets) == 1:
        steps = (("fwd", 0), ("in", 0), ("mid", 0), ("out", 0), ("red", 0))
    for stage, i in steps:
        stages[stage](i)

    for k in range(1, chips):
        src = lax.rem(chip + k, chips)
        remote(
            rs_recv.at[src], rs_recv.at[src], rs_ssem.at[0], rs_rsem.at[src], (partner, tp)
        ).wait_recv()
    result = state_buf[:, cols] + jnp.sum(rs_recv[...].astype(f32), axis=0)
    out_ref[...] = result.astype(bf16)
    for c in sends:
        c.wait_send()


def plan(chips):
    planes = PLANES
    if chips % (2 * planes):
        return ((chips, lambda chip: 0, False, True),)
    deep = chips // planes
    half = deep // 2

    def other(k):
        return lambda chip: (chip // deep ^ k) * deep

    return (
        (half, lambda chip: chip // half * half, False, True),
        (half, lambda chip: (chip // half ^ 1) * half, True, False),
    ) + tuple((deep, other(k), False, False) for k in FAR)


def layer_call(
    q, nk, nv, cum, flogit, fbias, lengths, resid, gain, mix, routes, route_weight, kc, vc, ow, eg,
    eu, ed, dg, du, dd,
):
    ep_n, tp_n = lax.axis_size("ep"), lax.axis_size("tp")
    chips = ep_n // 2
    sets = plan(chips)
    tokens, full = resid.shape
    width = full // tp_n
    rows = ep_n * tokens
    whole = 2 * sets[0][0] * tokens
    count = len(sets)
    span, dspan = eg.shape[2], dg.shape[0]
    hidden = span + dspan
    assert ep_n // EXP_SPAN + 1 <= SEG
    f32, bf16 = jnp.float32, jnp.bfloat16
    heads = cum.shape[1]
    vmem = pl.BlockSpec(memory_space=pltpu.VMEM)
    hbm = pl.BlockSpec(memory_space=pl.ANY)
    dma = pltpu.SemaphoreType.DMA
    peers = max(tp_n - 1, 1)
    return pl.pallas_call(
        functools.partial(layer_kernel, (ep_n, tp_n, sets)),
        out_shape=pltpu.VMEM((tokens, width), bf16),
        in_specs=[hbm] * 21,
        out_specs=vmem,
        scratch_shapes=[
            pltpu.VMEM(q.shape, bf16),
            pltpu.VMEM(nk.shape, bf16),
            pltpu.VMEM(nv.shape, bf16),
            pltpu.VMEM(cum.shape, f32),
            pltpu.VMEM(flogit.shape, f32),
            pltpu.SMEM(fbias.shape, f32),
            pltpu.SMEM(lengths.shape, jnp.int32),
            pltpu.VMEM(resid.shape, bf16),
            pltpu.VMEM(gain.shape, f32),
            pltpu.VMEM(mix.shape, bf16),
            pltpu.VMEM(routes.shape, jnp.int32),
            pltpu.VMEM(route_weight.shape, f32),
            pltpu.VMEM(kc.shape, bf16),
            pltpu.VMEM(vc.shape, bf16),
            pltpu.VMEM((tokens, heads, nk.shape[1]), f32),
            pltpu.VMEM((tokens, heads, nk.shape[1]), f32),
            pltpu.VMEM((tokens, heads, HEAD), f32),
            pltpu.VMEM((tokens, heads, HEAD), f32),
            pltpu.VMEM((tokens, heads, HEAD), jnp.int32),
            pltpu.VMEM(cum.shape, f32),
            pltpu.VMEM(cum.shape, f32),
            pltpu.VMEM((tokens, heads, HEAD), f32),
            pltpu.VMEM((tokens, heads * HEAD), bf16),
            pltpu.VMEM(ow.shape, bf16),
            pltpu.VMEM((width, 2 * hidden), bf16),
            pltpu.VMEM((hidden, width), bf16),
            pltpu.VMEM((2 * dspan, width), bf16),
            pltpu.VMEM((tokens, full), bf16),
            pltpu.VMEM((peers, tokens, full), bf16),
            pltpu.VMEM((tokens, full), f32),
            pltpu.VMEM((tokens, full), f32),
            pltpu.VMEM((2, chips, tokens, width + META), bf16),
            pltpu.VMEM((rows // tp_n, 2 * hidden), f32),
            pltpu.VMEM((peers, rows // tp_n, 2 * hidden), bf16),
            pltpu.VMEM((peers, rows // tp_n, 2 * hidden), bf16),
            pltpu.VMEM((whole, 2 * hidden), f32),
            pltpu.VMEM((whole, 2 * hidden), bf16),
            pltpu.VMEM((peers, whole, 2 * hidden), bf16),
            pltpu.VMEM((rows, hidden), bf16),
            pltpu.VMEM((2, rows // 2, width), f32),
            pltpu.VMEM((rows // 2, width), bf16),
            pltpu.VMEM((rows // 2, width), bf16),
            pltpu.VMEM((chips, tokens, width), bf16),
            pltpu.VMEM((chips, tokens, width), bf16),
            dma((12,)),
            dma((7,)),
            dma((2, CACHE_CHUNKS)),
            dma((peers,)),
            dma((peers,)),
            dma((3 * chips,)),
            dma((1,)),
            dma((2, chips)),
            dma((count, peers)),
            dma((count, peers)),
            dma((count, peers)),
            dma((count, peers)),
            dma((count,)),
            dma((count,)),
            dma((chips,)),
            dma((chips,)),
        ],
        compiler_params=pltpu.CompilerParams(
            collective_id=0, has_side_effects=True, vmem_limit_bytes=VMEM_LIMIT
        ),
        name="layer",
    )(
        q, nk, nv, cum, flogit, fbias, lengths, resid, gain, mix, routes, route_weight, kc, vc, ow,
        eg, eu, ed, dg, du, dd,
    )


def body(
    resid,
    queries,
    new_keys,
    new_values,
    key_cache,
    value_cache,
    cum_gate,
    forget_logit,
    forget_bias,
    lengths,
    out_weight,
    norm_gain,
    mix_vector,
    routes,
    route_weight,
    expert_gate,
    expert_up,
    expert_down,
    dense_gate,
    dense_up,
    dense_down,
):
    result = layer_call(
        queries,
        new_keys,
        new_values,
        cum_gate,
        forget_logit.T,
        forget_bias,
        lengths,
        resid,
        norm_gain.reshape(1, -1),
        mix_vector.reshape(-1, HEAD),
        routes.T,
        route_weight.T,
        key_cache,
        value_cache,
        out_weight,
        expert_gate,
        expert_up,
        expert_down,
        dense_gate.T,
        dense_up.T,
        dense_down,
    )
    return result


def solution(mesh):
    placed = (
        P("ep", None),
        P("ep", "tp"),
        P("ep", "tp"),
        P("ep", "tp"),
        P("ep", "tp", None, None),
        P("ep", "tp", None, None),
        P("ep", "tp", None),
        P("ep", "tp"),
        P("tp"),
        P("ep"),
        P("tp", None),
        P(),
        P(),
        P("ep", None),
        P("ep", None),
        P("ep", "tp", None),
        P("ep", "tp", None),
        P("ep", None, "tp"),
        P("tp", "ep"),
        P("tp", "ep"),
        P("ep", "tp"),
    )
    return jax.shard_map(body, mesh=mesh, in_specs=placed, out_specs=P("ep", "tp"), check_vma=False)
```

time: 41.5 us -> 40.7 us (0.981)
  Pallas kernels: 40.7 us -> 39.9 us
    pallas_call x1, Pallas kernels: 40.7 us -> 39.9 us  [layer_call(): pl.pallas_call(functools.partial(layer_kernel, (ep_n, tp_n, sets)), out_s...]
where the time goes in v2:
time: 40.7 us; the launch traced here: 40.5 us
  Pallas kernels  39.9 us (98%)
  local copies, waits for them, and re-layouts  0.62 us (2%)
    pallas_call x1, Pallas kernels, layer_call(): pl.pallas_call(functools.partial(layer_kernel, (ep_n, tp_n, sets)), out_s...  39.9 us

profile of v2, /device:TPU:0, one launch (start us, length us, event | category | flops | bytes accessed | tf_op | source)
XLA Modules:
  0.0 40.5 jit_solution(3906083861783130680)
XLA Ops:
  0.0 39.9 %layer.1 = bf16[16,1024]{1,0:T(8,128)(2,1)S(1)} custom-call(bf16[16,512]{1,0:T(8,128)(2,1)} %q_hbm.1, bf16[16,256]{1,0:T(8,128)(2,1)} %nk_hbm.1, bf16[16,256]{1,0:T(8,128)(2,1)} %nv_hbm.1, f32[16,4,256]{2,1,0:T(4,128)} %cum_hbm.1, f32[4,16]{1,0:T(4,128)} %bitcast.11, f32[4]{0:T(128)} %fbias_hbm.1, s32[16]{0:T(128)} %len_hbm.1, bf16[16,2048]{1,0:T(8,128)(2,1)} %resid_hbm.1, ...), custom_call_target="tpu_custom_call" | custom-call | tf_op jit(solution)/shard_map/layer/pallas_call | solution.py:618
  39.9 0.6 %copy.23 = bf16[16,1024]{1,0:T(8,128)(2,1)} copy(bf16[16,1024]{1,0:T(8,128)(2,1)S(1)} %layer.1) | data formatting | bytes 65536

commit v3 on v2

--- a/solution.py
+++ b/solution.py
@@ -18,7 +18,9 @@
 META = 128
 SEG = 42
 PLANES = 4
-FAR = (1, 2, 3)
+ORDER = ((1, 2, 3), (0, 3, 2), (0, 3, 1), (0, 2, 1))
+SENDS = ((2, 3, 1), (0, 2, 3), (1, 3, 0), (1, 2, 0))
+SPLIT = (2,)
 STEPS = (
     ("fwd", 0),
     ("in", 0),
@@ -31,6 +33,8 @@
     ("fwd", 4),
     ("mid", 2),
     ("in", 4),
+    ("fwd", 5),
+    ("in", 5),
     ("mid", 0),
     ("out", 1),
     ("red", 1),
@@ -40,10 +44,13 @@
     ("out", 2),
     ("mid", 4),
     ("red", 2),
+    ("mid", 5),
     ("out", 3),
     ("red", 3),
     ("out", 4),
     ("red", 4),
+    ("out", 5),
+    ("red", 5),
 )
 CACHE_CHUNKS = 4
 VMEM_LIMIT = 60 * 1024 * 1024
@@ -123,7 +130,6 @@
     pp_ssem,
     pp_rsem,
     ag_ssem,
-    ag_psem,
     ag_rsem,
     p_ssem,
     p_rsem,
@@ -134,7 +140,7 @@
     rs_ssem,
     rs_rsem,
 ):
-    ep_n, tp_n, sets = dims
+    ep_n, tp_n, sets, sent = dims
     ep = lax.axis_index("ep")
     tp = lax.axis_index("tp")
     f32, bf16 = jnp.float32, jnp.bfloat16
@@ -162,7 +168,7 @@
                 pltpu.make_async_copy(src.at[some], dst.at[some], cache_sem.at[side, n])
             )
     smalls = [
-        pltpu.make_async_copy(src, dst, small_sem.at[i])
+        pltpu.make_async_copy(src, dst, small_sem.at[i % 7])
         for i, (src, dst) in enumerate(
             [
                 (q_hbm, q_ref),
@@ -187,22 +193,18 @@
     for load in cache[1:]:
         load.start()
     loads = [
-        pltpu.make_async_copy(src, dst, load_sem.at[i])
-        for i, (src, dst) in enumerate(
-            [
-                (ow_hbm, ow),
-                (dg_hbm, dgu.at[0:dspan]),
-                (du_hbm, dgu.at[dspan : 2 * dspan]),
-                (eg_hbm.at[0], wgu.at[:, 0:span]),
-                (eu_hbm.at[0], wgu.at[:, span : 2 * span]),
-                (ed_hbm.at[0], wd.at[0:span]),
-                (dd_hbm, wd.at[span:hidden]),
-            ]
-        )
+        pltpu.make_async_copy(src, dst, sem)
+        for src, dst, sem in [
+            (ow_hbm, ow, load_sem.at[0]),
+            (dg_hbm, dgu.at[0:dspan], cache_sem.at[0, 0]),
+            (du_hbm, dgu.at[dspan : 2 * dspan], cache_sem.at[0, 1]),
+            (eg_hbm.at[0], wgu.at[:, 0:span], cache_sem.at[0, 2]),
+            (eu_hbm.at[0], wgu.at[:, span : 2 * span], cache_sem.at[0, 3]),
+            (ed_hbm.at[0], wd.at[0:span], cache_sem.at[1, 0]),
+            (dd_hbm, wd.at[span:hidden], cache_sem.at[1, 1]),
+        ]
     ]
     loads[0].start()
-    for load in smalls[7:]:
-        load.start()
 
     barrier = pltpu.get_barrier_semaphore()
     for k in range(1, ep_n):
@@ -234,6 +236,8 @@
         lf_buf[:, h, :] = jnp.broadcast_to(
             jnp.minimum(x, 0.0) - jnp.log1p(jnp.exp(-jnp.abs(x))), (tokens, HEAD)
         )
+    for load in smalls[7:]:
+        load.start()
     head_row = lax.broadcasted_iota(jnp.int32, (heads, HEAD), 0)
     for n in range(tokens):
         len_buf[n] = jnp.full((heads, HEAD), len_ref[n], jnp.int32)
@@ -260,7 +264,7 @@
             (((1,), (1,)), ((), ())),
             preferred_element_type=f32,
         )
-    for load in loads[1:]:
+    for load in loads[1:5]:
         load.start()
     scores = score_buf[...] * scale + add_buf[...]
     highest = jnp.maximum(jnp.max(scores, axis=2, keepdims=True), own)
@@ -279,6 +283,8 @@
                 head_row >= g * grouping, both[:, g * HEAD : (g + 1) * HEAD], taken
             )
         mix_buf[n] = taken
+    for load in loads[5:7]:
+        load.start()
     mix_buf[...] = mix_buf[...] + own_prob * nv_buf[...]
     for h in range(heads):
         att_buf[:, h * HEAD : (h + 1) * HEAD] = mix_buf[:, h, :].astype(bf16)
@@ -332,7 +338,7 @@
     state_buf[...] = state_full
     norm_buf[...] = scaled_full * inverse
     cols = pl.ds(pl.multiple_of(tp * width, 128), width)
-    gat[core, chip, :, 0:width] = norm_buf[:, cols].astype(bf16)
+    gat[core * chips + chip, :, 0:width] = norm_buf[:, cols].astype(bf16)
     lane = lax.broadcasted_iota(jnp.int32, (tokens, META), 1)
     named = [column(routes_ref[k : k + 1, :].astype(f32)) for k in range(TOP_K)]
     weighed = [column(rw_ref[k : k + 1, :]) for k in range(TOP_K)]
@@ -348,16 +354,15 @@
         for cut in range(s):
             value = value - value.astype(bf16).astype(f32)
         meta = meta + value
-    gat[core, chip, :, width : width + META] = meta.astype(bf16)
+    gat[core * chips + chip, :, width : width + META] = meta.astype(bf16)
 
     def put(src, dst, ssem, rsem, to):
         c = remote(src, dst, ssem, rsem, to)
         c.start()
-        sends.append(c)
         return c
 
-    block = gat.at[core, chip]
-    put(block, block, ag_psem.at[0], ag_rsem.at[core, chip], (partner, tp))
+    block = gat.at[core * chips + chip]
+    gathers = [put(block, block, ag_ssem.at[0], ag_rsem.at[core, chip], (partner, tp))]
 
     def others(i):
         count, where, direct, whole = sets[i]
@@ -367,34 +372,31 @@
                 continue
             yield first + lax.rem(chip + b, count) if count > 1 else first
 
-    number = [0]
-
-    def spot():
-        number[0] += 1
-        return number[0] - 1
-
-    for i in range(len(sets)):
+    def give(one, side, there, to):
+        gathers.append(put(one, one, ag_ssem.at[0], ag_rsem.at[side, there], (to, tp)))
+
+    for i in range(min(2, len(sets))):
         for there in others(i):
-            put(block, block, ag_ssem.at[spot()], ag_rsem.at[core, chip], (there * 2 + core, tp))
+            give(block, core, chip, there * 2 + core)
             if sets[i][2]:
-                put(
-                    block,
-                    block,
-                    ag_ssem.at[spot()],
-                    ag_rsem.at[core, chip],
-                    (there * 2 + 1 - core, tp),
-                )
+                give(block, core, chip, there * 2 + 1 - core)
+    if sent is not None:
+        deep = chips // PLANES
+        for k in range(PLANES - 1):
+            for b in range(deep):
+                there = sent(k, chip) + lax.rem(chip + b, deep)
+                give(block, core, chip, there * 2 + core)
 
     def arrive(side, there):
-        came = gat.at[side, there]
-        remote(came, came, ag_psem.at[0], ag_rsem.at[side, there], (partner, tp)).wait_recv()
+        came = gat.at[side * chips + there]
+        remote(came, came, ag_ssem.at[0], ag_rsem.at[side, there], (partner, tp)).wait_recv()
 
     def forward(i):
         for there in others(i):
             arrive(core, there)
-            came = gat.at[core, there]
+            came = gat.at[core * chips + there]
             if not sets[i][2]:
-                put(came, came, ag_ssem.at[spot()], ag_rsem.at[core, there], (partner, tp))
+                give(came, core, there, partner)
 
     pcopies = {}
     hcopies = {}
@@ -405,11 +407,11 @@
         count, where, direct, whole = sets[i]
         share = 2 * count // tp_n
         at = k * share
-        return gat.at[at // count, pl.ds(where(chip) + lax.rem(at, count), share)]
+        return gat.at[pl.ds(at // count * chips + where(chip) + lax.rem(at, count), share)]
 
     def everything(i):
         count, where, direct, whole = sets[i]
-        return [gat.at[side, pl.ds(where(chip), count)] for side in range(2)]
+        return [gat.at[pl.ds(side * chips + where(chip), count)] for side in range(2)]
 
     def stage_in(i):
         count, where, direct, whole = sets[i]
@@ -447,7 +449,7 @@
                 put(
                     src,
                     dst,
-                    p_ssem.at[i, k - 1],
+                    p_ssem.at[int(whole), k - 1],
                     p_rsem.at[i, k - 1],
                     (ep, lax.rem(tp + k, tp_n)),
                 )
@@ -502,14 +504,14 @@
             return
         for k in range(1, tp_n):
             to = lax.rem(tp + k, tp_n)
-            put(hid.at[mine], hid.at[mine], h_ssem.at[i, k - 1], h_rsem.at[i, k - 1], (ep, to))
+            put(hid.at[mine], hid.at[mine], h_ssem.at[k - 1], h_rsem.at[i, k - 1], (ep, to))
             source = lax.rem(tp + tp_n - k, tp_n)
             theirs = pl.ds(pl.multiple_of(firsts[i] + source * part, 16), part)
             hcopies[i].append(
                 remote(
                     hid.at[theirs],
                     hid.at[theirs],
-                    h_ssem.at[i, k - 1],
+                    h_ssem.at[k - 1],
                     h_rsem.at[i, k - 1],
                     (ep, to),
                 )
@@ -531,7 +533,7 @@
         outs[1, at] = value[half : 2 * half]
         cs_send[at] = outs[1 - core, at].astype(bf16)
         ccopies[i] = put(
-            cs_send.at[at], cs_recv.at[at], c_ssem.at[i], c_rsem.at[i], (partner, tp)
+            cs_send.at[at], cs_recv.at[at], c_ssem.at[0], c_rsem.at[i], (partner, tp)
         )
 
     def stage_red(i):
@@ -549,8 +551,8 @@
             put(
                 rs_send.at[first + slot],
                 rs_recv.at[chip],
-                rs_ssem.at[first + b],
-                rs_rsem.at[chip],
+                rs_ssem.at[0],
+                rs_rsem.at[0],
                 ((where(chip) + slot) * 2 + core, tp),
             )
 
@@ -567,31 +569,50 @@
     for stage, i in steps:
         stages[stage](i)
 
-    for k in range(1, chips):
-        src = lax.rem(chip + k, chips)
-        remote(
-            rs_recv.at[src], rs_recv.at[src], rs_ssem.at[0], rs_rsem.at[src], (partner, tp)
-        ).wait_recv()
+    def same(ref, ssem, rsem):
+        return remote(ref, ref, ssem, rsem, (partner, tp))
+
+    theirs = same(rs_recv.at[0 : chips - 1], rs_ssem.at[0], rs_rsem.at[0])
+    theirs.wait_recv()
     result = state_buf[:, cols] + jnp.sum(rs_recv[...].astype(f32), axis=0)
     out_ref[...] = result.astype(bf16)
+    theirs.wait_send()
     for c in sends:
         c.wait_send()
+    same(gat.at[0 : len(gathers)], ag_ssem.at[0], ag_rsem.at[0, 0]).wait_send()
+    same(cs_send, c_ssem.at[0], c_rsem.at[0]).wait_send()
+    rest = (sum(sizes) - sizes[0]) // tp_n
+    for k in range(tp_n - 1):
+        same(asend, p_ssem.at[1, k], p_rsem.at[0, k]).wait_send()
+        if rest:
+            same(psend.at[k, 0:rest], p_ssem.at[0, k], p_rsem.at[0, k]).wait_send()
+            same(hid.at[0:rest], h_ssem.at[k], h_rsem.at[0, k]).wait_send()
 
 
 def plan(chips):
     planes = PLANES
     if chips % (2 * planes):
-        return ((chips, lambda chip: 0, False, True),)
+        return ((chips, lambda chip: 0, False, True),), None
     deep = chips // planes
     half = deep // 2
 
-    def other(k):
-        return lambda chip: (chip // deep ^ k) * deep
-
-    return (
+    def pick(table, k, chip):
+        return sum(jnp.where(chip // deep == p, table[p][k], 0) for p in range(planes))
+
+    def other(k, at):
+        return lambda chip: pick(ORDER, k, chip) * deep + at
+
+    sets = [
         (half, lambda chip: chip // half * half, False, True),
         (half, lambda chip: (chip // half ^ 1) * half, True, False),
-    ) + tuple((deep, other(k), False, False) for k in FAR)
+    ]
+    for k in range(planes - 1):
+        if k in SPLIT:
+            sets.append((half, other(k, 0), False, False))
+            sets.append((half, other(k, half), False, False))
+        else:
+            sets.append((deep, other(k, 0), False, False))
+    return tuple(sets), lambda k, chip: pick(SENDS, k, chip) * deep
 
 
 def layer_call(
@@ -600,7 +621,7 @@
 ):
     ep_n, tp_n = lax.axis_size("ep"), lax.axis_size("tp")
     chips = ep_n // 2
-    sets = plan(chips)
+    sets, sent = plan(chips)
     tokens, full = resid.shape
     width = full // tp_n
     rows = ep_n * tokens
@@ -616,7 +637,7 @@
     dma = pltpu.SemaphoreType.DMA
     peers = max(tp_n - 1, 1)
     return pl.pallas_call(
-        functools.partial(layer_kernel, (ep_n, tp_n, sets)),
+        functools.partial(layer_kernel, (ep_n, tp_n, sets, sent)),
         out_shape=pltpu.VMEM((tokens, width), bf16),
         in_specs=[hbm] * 21,
         out_specs=vmem,
@@ -652,7 +673,7 @@
             pltpu.VMEM((peers, tokens, full), bf16),
             pltpu.VMEM((tokens, full), f32),
             pltpu.VMEM((tokens, full), f32),
-            pltpu.VMEM((2, chips, tokens, width + META), bf16),
+            pltpu.VMEM((2 * chips, tokens, width + META), bf16),
             pltpu.VMEM((rows // tp_n, 2 * hidden), f32),
             pltpu.VMEM((peers, rows // tp_n, 2 * hidden), bf16),
             pltpu.VMEM((peers, rows // tp_n, 2 * hidden), bf16),
@@ -665,22 +686,21 @@
             pltpu.VMEM((rows // 2, width), bf16),
             pltpu.VMEM((chips, tokens, width), bf16),
             pltpu.VMEM((chips, tokens, width), bf16),
-            dma((12,)),
             dma((7,)),
+            dma((1,)),
             dma((2, CACHE_CHUNKS)),
             dma((peers,)),
             dma((peers,)),
-            dma((3 * chips,)),
             dma((1,)),
             dma((2, chips)),
+            dma((2, peers)),
             dma((count, peers)),
+            dma((peers,)),
             dma((count, peers)),
-            dma((count, peers)),
-            dma((count, peers)),
+            dma((1,)),
             dma((count,)),
-            dma((count,)),
-            dma((chips,)),
-            dma((chips,)),
+            dma((1,)),
+            dma((1,)),
         ],
         compiler_params=pltpu.CompilerParams(
             collective_id=0, has_side_effects=True, vmem_limit_bytes=VMEM_LIMIT

time: 40.7 us -> 38.9 us (0.956)
  the two profiles are of different devices: /device:TPU:0 before, /device:TPU:21 now
where the time goes in v3:
time: 38.9 us; the launch traced here: 38.7 us
  Pallas kernels  38.1 us (98%)
  local copies, waits for them, and re-layouts  0.62 us (2%)
    pallas_call x1, Pallas kernels, layer_call(): pl.pallas_call(functools.partial(layer_kernel, (ep_n, tp_n, sets, sent)),...  38.1 us

profile of v3, /device:TPU:21, one launch (start us, length us, event | category | flops | bytes accessed | tf_op | source)
XLA Modules:
  0.0 38.7 jit_solution(17124556457216998393)
XLA Ops:
  0.0 38.1 %layer.1 = bf16[16,1024]{1,0:T(8,128)(2,1)S(1)} custom-call(bf16[16,512]{1,0:T(8,128)(2,1)} %q_hbm.1, bf16[16,256]{1,0:T(8,128)(2,1)} %nk_hbm.1, bf16[16,256]{1,0:T(8,128)(2,1)} %nv_hbm.1, f32[16,4,256]{2,1,0:T(4,128)} %cum_hbm.1, f32[4,16]{1,0:T(4,128)} %bitcast.11, f32[4]{0:T(128)} %fbias_hbm.1, s32[16]{0:T(128)} %len_hbm.1, bf16[16,2048]{1,0:T(8,128)(2,1)} %resid_hbm.1, ...), custom_call_target="tpu_custom_call" | custom-call | tf_op jit(solution)/shard_map/layer/pallas_call | solution.py:639
  38.1 0.6 %copy.23 = bf16[16,1024]{1,0:T(8,128)(2,1)} copy(bf16[16,1024]{1,0:T(8,128)(2,1)S(1)} %layer.1) | data formatting | bytes 65536

commit v4 on v3

--- a/solution.py
+++ b/solution.py
@@ -31,9 +31,9 @@
     ("mid", 1),
     ("in", 3),
     ("fwd", 4),
-    ("mid", 2),
     ("in", 4),
     ("fwd", 5),
+    ("mid", 2),
     ("in", 5),
     ("mid", 0),
     ("out", 1),
@@ -41,10 +41,10 @@
     ("mid", 3),
     ("out", 0),
     ("red", 0),
+    ("mid", 4),
     ("out", 2),
-    ("mid", 4),
+    ("mid", 5),
     ("red", 2),
-    ("mid", 5),
     ("out", 3),
     ("red", 3),
     ("out", 4),
@@ -168,7 +168,7 @@
                 pltpu.make_async_copy(src.at[some], dst.at[some], cache_sem.at[side, n])
             )
     smalls = [
-        pltpu.make_async_copy(src, dst, small_sem.at[i % 7])
+        pltpu.make_async_copy(src, dst, small_sem.at[i])
         for i, (src, dst) in enumerate(
             [
                 (q_hbm, q_ref),
@@ -205,6 +205,8 @@
         ]
     ]
     loads[0].start()
+    for load in smalls[7:]:
+        load.start()
 
     barrier = pltpu.get_barrier_semaphore()
     for k in range(1, ep_n):
@@ -236,8 +238,6 @@
         lf_buf[:, h, :] = jnp.broadcast_to(
             jnp.minimum(x, 0.0) - jnp.log1p(jnp.exp(-jnp.abs(x))), (tokens, HEAD)
         )
-    for load in smalls[7:]:
-        load.start()
     head_row = lax.broadcasted_iota(jnp.int32, (heads, HEAD), 0)
     for n in range(tokens):
         len_buf[n] = jnp.full((heads, HEAD), len_ref[n], jnp.int32)
@@ -283,8 +283,6 @@
                 head_row >= g * grouping, both[:, g * HEAD : (g + 1) * HEAD], taken
             )
         mix_buf[n] = taken
-    for load in loads[5:7]:
-        load.start()
     mix_buf[...] = mix_buf[...] + own_prob * nv_buf[...]
     for h in range(heads):
         att_buf[:, h * HEAD : (h + 1) * HEAD] = mix_buf[:, h, :].astype(bf16)
@@ -317,6 +315,8 @@
         c.start()
         pp.append(c)
         sends.append(c)
+    for load in loads[5:7]:
+        load.start()
     for load in smalls[7:]:
         load.wait()
     loads[1].wait()
@@ -686,7 +686,7 @@
             pltpu.VMEM((rows // 2, width), bf16),
             pltpu.VMEM((chips, tokens, width), bf16),
             pltpu.VMEM((chips, tokens, width), bf16),
-            dma((7,)),
+            dma((12,)),
             dma((1,)),
             dma((2, CACHE_CHUNKS)),
             dma((peers,)),

time: 38.9 us -> 38.1 us (0.979)
  the two profiles are of different devices: /device:TPU:21 before, /device:TPU:0 now
where the time goes in v4:
time: 38.1 us; the launch traced here: 37.6 us
  Pallas kernels  37 us (97%)
  local copies, waits for them, and re-layouts  0.62 us (2%)
    pallas_call x1, Pallas kernels, layer_call(): pl.pallas_call(functools.partial(layer_kernel, (ep_n, tp_n, sets, sent)),...  37 us

profile of v4, /device:TPU:0, one launch (start us, length us, event | category | flops | bytes accessed | tf_op | source)
XLA Modules:
  0.0 37.6 jit_solution(13841633605223661867)
XLA Ops:
  0.0 37.0 %layer.1 = bf16[16,1024]{1,0:T(8,128)(2,1)S(1)} custom-call(bf16[16,512]{1,0:T(8,128)(2,1)} %q_hbm.1, bf16[16,256]{1,0:T(8,128)(2,1)} %nk_hbm.1, bf16[16,256]{1,0:T(8,128)(2,1)} %nv_hbm.1, f32[16,4,256]{2,1,0:T(4,128)} %cum_hbm.1, f32[4,16]{1,0:T(4,128)} %bitcast.11, f32[4]{0:T(128)} %fbias_hbm.1, s32[16]{0:T(128)} %len_hbm.1, bf16[16,2048]{1,0:T(8,128)(2,1)} %resid_hbm.1, ...), custom_call_target="tpu_custom_call" | custom-call | tf_op jit(solution)/shard_map/layer/pallas_call | solution.py:639
  37.0 0.6 %copy.23 = bf16[16,1024]{1,0:T(8,128)(2,1)} copy(bf16[16,1024]{1,0:T(8,128)(2,1)S(1)} %layer.1) | data formatting | bytes 65536
